TPU v7x, 32 devices: a whole 2x2x4 slice. The times are simulated.
32 devices in a mesh: grp: 2 (over y), ep: 4 (over z), tp: 4 (over x, core).
Axes of the slice: x: 2, y: 2, z: 4, core: 2. Of those that a mesh axis runs over, the one named last changes fastest.
Arguments:
- queries: bfloat16 [1024, 16, 128], P(('grp', 'ep'), 'tp'), parts along dimension 0, may hold values from -6 to 6
- key_vectors: bfloat16 [1024, 16, 128], P(('grp', 'ep'), 'tp'), parts along dimension 0, may hold values from -6 to 6
- values: bfloat16 [1024, 16, 128], P(('grp', 'ep'), 'tp'), parts along dimension 0, may hold values from -6 to 6
- forget_cum: float32 [1024, 16], P('grp', 'tp'), parts along dimension 0, may hold values from -90 to 0, as said below
- query_gain: float32 [128], replicated, may hold values from 0.1 to 5.5
- key_gain: float32 [128], replicated, may hold values from 0.1 to 5.5
- tokens: bfloat16 [4096, 4096], P(('grp', 'ep', 'tp')), parts along dimension 0, may hold values from -6 to 6
- norm_gain: float32 [4096], replicated, may hold values from 0.1 to 1.9
- routes: int32 [4096, 2], P(('grp', 'ep', 'tp')), parts along dimension 0, may hold values from 0 to 127, all different within a row; in each aligned block of 128 rows (0 to 127, 128 to 255, ...) at most 2 rows name the same one
- route_weights: float32 [4096, 2], P(('grp', 'ep', 'tp')), parts along dimension 0, may hold values from 0.3 to 1.2
- expert_gate: bfloat16 [128, 4096, 384], P(('ep', 'tp')), may hold values from -0.09375 to 0.09375
- expert_up: bfloat16 [128, 4096, 384], P(('ep', 'tp')), may hold values from -0.09375 to 0.09375
- expert_down: bfloat16 [128, 384, 4096], P(('ep', 'tp')), may hold values from -0.3125 to 0.3125
- shared_gate: bfloat16 [4096, 192], P(None, 'tp'), may hold values from -0.09375 to 0.09375
- shared_up: bfloat16 [4096, 192], P(None, 'tp'), may hold values from -0.09375 to 0.09375
- shared_down: bfloat16 [192, 4096], P('tp'), may hold values from -0.4375 to 0.4375
Outputs:
- attended: bfloat16 [1024, 16, 128], P(('grp', 'ep'), 'tp'), parts along dimension 0
- routed_output: bfloat16 [4096, 4096], P(('grp', 'ep', 'tp')), parts along dimension 0
There are 2 independent parts, one for each index of `grp`. A program takes and returns all parts, laid end to end along the dimension named above; an argument that names none is the same for every part. Nothing has to cross between parts.
Inputs may be any that keep to these rules, and one draw needn't show every extreme that they name: `routes`: each row names 2 different experts; the rows of one device name every expert exactly 2 times. `forget_cum`: never rises from one position to the next.
All inputs are finite; a program needn't handle non-finite values.
Results may differ from a plain program's by a relative error of at most 0.007.
The roundings to bfloat16 on the way count: a program that leaves them out, or rounds other values in their place, can miss the bound.
Values may be sent and summed in bfloat16 or wider, within the bound.
A program may use at most 128 MiB of HBM per device.

v0:
```python
import jax
import jax.numpy as jnp
from jax import lax
from jax.sharding import PartitionSpec as P

D = 4096
EXPERTS = 128
TOP_K = 2
CAP = 2


def rms_rows(row_values, gain_vector):
    widened = row_values.astype(jnp.float32)
    inverse = lax.rsqrt(jnp.mean(widened * widened, axis=-1, keepdims=True) + 1e-06)
    return (widened * inverse * gain_vector).astype(jnp.bfloat16)


def attend(queries, key_vectors, values, forget_cum, query_gain, key_gain):
    query_norm = rms_rows(queries, query_gain)
    key_norm = rms_rows(key_vectors, key_gain)
    query_rows = query_norm.shape[0]
    head_count = query_norm.shape[1]
    head_size = query_norm.shape[2]
    first_query = lax.axis_index("ep") * query_rows
    query_positions = first_query + lax.iota(jnp.int32, query_rows)
    last_query = first_query + query_rows - 1
    query_cum = lax.dynamic_slice_in_dim(forget_cum, first_query, query_rows, 0).T
    scale_factor = head_size ** (-0.5)
    start_state = (
        jnp.full((head_count, query_rows), -1e30, jnp.float32),
        jnp.zeros((head_count, query_rows), jnp.float32),
        jnp.zeros((head_count, query_rows, head_size), jnp.float32),
    )
    key_part = lax.all_gather(key_norm, "ep", axis=0, tiled=True)
    value_part = lax.all_gather(values, "ep", axis=0, tiled=True)
    piece_rows = key_part.shape[0]

    def compute(inner_state):
        best_score, denominator, accumulated = inner_state
        cum_block = forget_cum.T
        scores = jnp.einsum(
            "qhd,khd->hqk", query_norm, key_part, preferred_element_type=jnp.float32
        )
        scores = scores * scale_factor + query_cum[:, :, None] - cum_block[:, None, :]
        key_positions = lax.iota(jnp.int32, piece_rows)
        allowed = (key_positions[None, :] <= query_positions[:, None])[None]
        scores = jnp.where(allowed, scores, -1e30)
        new_best = jnp.maximum(best_score, jnp.max(scores, axis=2))
        weights = jnp.where(allowed, jnp.exp(scores - new_best[:, :, None]), 0.0)
        denominator = jnp.sum(weights, axis=2)
        product = jnp.einsum(
            "hqk,khd->hqd",
            weights.astype(jnp.bfloat16),
            value_part,
            preferred_element_type=jnp.float32,
        )
        accumulated = product
        return (new_best, denominator, accumulated)

    best_score, denominator, accumulated = lax.cond(
        jnp.int32(0) <= last_query, compute, lambda inner_state: inner_state, start_state
    )
    return (accumulated / denominator[:, :, None]).transpose(1, 0, 2).astype(jnp.bfloat16)


def shared_expert(normed, shared_gate, shared_up, shared_down):
    row_count = normed.shape[0]
    whole_gate, whole_up, whole_down = (
        lax.all_gather(shared_gate, "tp", axis=1, tiled=True),
        lax.all_gather(shared_up, "tp", axis=1, tiled=True),
        lax.all_gather(shared_down, "tp", axis=0, tiled=True),
    )
    block_total = lax.axis_size("tp")
    gate_values = jnp.dot(normed, whole_gate, preferred_element_type=jnp.float32)
    upward = jnp.dot(normed, whole_up, preferred_element_type=jnp.float32)
    hidden_whole = (jax.nn.silu(gate_values) * upward).astype(jnp.bfloat16)
    part_width = whole_down.shape[0] // block_total
    hidden_blocks = hidden_whole.reshape(row_count, block_total, part_width)
    down_blocks = whole_down.reshape(block_total, part_width, whole_down.shape[1])
    partials = jnp.einsum(
        "rnp,npd->nrd", hidden_blocks, down_blocks, preferred_element_type=jnp.float32
    ).astype(jnp.bfloat16)
    return jnp.sum(partials.astype(jnp.float32), axis=0).astype(jnp.bfloat16)


def mixture(
    tokens,
    norm_gain,
    routes,
    route_weights,
    expert_gate,
    expert_up,
    expert_down,
    shared_gate,
    shared_up,
    shared_down,
):
    normed = rms_rows(tokens, norm_gain)
    row_count = tokens.shape[0]
    shared_out = shared_expert(normed, shared_gate, shared_up, shared_down)
    flat_routes = routes.reshape(-1)
    choice_count = flat_routes.shape[0]
    one_hot = (flat_routes[:, None] == lax.iota(jnp.int32, EXPERTS)[None, :]).astype(jnp.int32)
    slot_rank = jnp.sum((jnp.cumsum(one_hot, axis=0) - one_hot) * one_hot, axis=1)
    slot_index = slot_rank * EXPERTS + flat_routes
    slot_ids = lax.iota(jnp.int32, CAP * EXPERTS)
    matches = slot_index[None, :] == slot_ids[:, None]
    source_row = jnp.sum(
        jnp.where(matches, lax.iota(jnp.int32, choice_count)[None, :] // TOP_K, 0), axis=1
    )
    filled = jnp.any(matches, axis=1)
    outgoing = jnp.where(filled[:, None], normed[source_row], jnp.zeros((), jnp.bfloat16)).reshape(
        CAP, EXPERTS, D
    )
    arrived = lax.all_to_all(outgoing, ("ep", "tp"), split_axis=1, concat_axis=1, tiled=True)
    local_count = expert_gate.shape[0]
    grouped = arrived.reshape(CAP, -1, local_count, D)
    gate_values = jnp.einsum(
        "csed,edf->csef", grouped, expert_gate, preferred_element_type=jnp.float32
    )
    upward = jnp.einsum("csed,edf->csef", grouped, expert_up, preferred_element_type=jnp.float32)
    hidden = (jax.nn.silu(gate_values) * upward).astype(jnp.bfloat16)
    produced = (
        jnp.einsum("csef,efd->csed", hidden, expert_down, preferred_element_type=jnp.float32)
        .astype(jnp.bfloat16)
        .reshape(CAP, -1, D)
    )
    returned = lax.all_to_all(produced, ("ep", "tp"), split_axis=1, concat_axis=1, tiled=True)
    picked_rows = returned.reshape(CAP * EXPERTS, D)[slot_index].reshape(row_count, TOP_K, D)
    routed = jnp.sum(route_weights[:, :, None] * picked_rows.astype(jnp.float32), axis=1)
    return (shared_out.astype(jnp.float32) + routed).astype(jnp.bfloat16)


def local(
    queries,
    key_vectors,
    values,
    forget_cum,
    query_gain,
    key_gain,
    tokens,
    norm_gain,
    routes,
    route_weights,
    expert_gate,
    expert_up,
    expert_down,
    shared_gate,
    shared_up,
    shared_down,
):
    attended = attend(queries, key_vectors, values, forget_cum, query_gain, key_gain)
    routed_output = mixture(
        tokens,
        norm_gain,
        routes,
        route_weights,
        expert_gate,
        expert_up,
        expert_down,
        shared_gate,
        shared_up,
        shared_down,
    )
    return (attended, routed_output)


def solution(mesh):
    placed = (
        P(("grp", "ep"), "tp", None),
        P(("grp", "ep"), "tp", None),
        P(("grp", "ep"), "tp", None),
        P("grp", "tp"),
        P(),
        P(),
        P(("grp", "ep", "tp"), None),
        P(),
        P(("grp", "ep", "tp"), None),
        P(("grp", "ep", "tp"), None),
        P(("ep", "tp"), None, None),
        P(("ep", "tp"), None, None),
        P(("ep", "tp"), None, None),
        P(None, "tp"),
        P(None, "tp"),
        P("tp", None),
    )
    return jax.shard_map(
        local,
        mesh=mesh,
        in_specs=placed,
        out_specs=(P(("grp", "ep"), "tp", None), P(("grp", "ep", "tp"), None)),
        check_vma=False,
    )
```

profile of v0, /device:TPU:0, one launch (start us, length us, event | category | flops | bytes accessed | tf_op | source)
XLA Modules:
  0.0 230.9 jit_solution(5048719747301511845)
XLA Ops:
  7.2 0.9 copy.80
  8.1 0.1 eq.42
  8.2 0.1 eq.38
  8.5 0.2 fusion.67
  8.8 0.2 fusion.69
  9.0 0.1 fusion.65
  9.1 0.1 select_reduce_fusion
  9.2 1.5 fusion.23
  10.8 0.1 copy.84
  10.9 0.3 fusion.25
  11.2 1.8 gather_fusion
  13.1 3.8 %broadcast_select_fusion = bf16[2,128,4096]{2,0,1:T(2,128)(2,1)} fusion(pred[2,128]{0,1:T(8,128)(4,1)S(1)} %copy.84, bf16[2,128,4096]{2,1,0:T(8,128)(2,1)S(1)} %bitcast.86), kind=kLoop, calls=%fused_computation.27 | loop fusion | flops 1048576 | bytes 4194560 | tf_op jit(solution)/shard_map/jit(_where)/select_n | solution.py:112
  16.9 7.4 %all-to-all-start = ((bf16[2,128,4096]{2,0,1:T(2,128)(2,1)}), bf16[2,128,4096]{2,0,1:T(2,128)(2,1)}, u32[]{:S(2)}, u32[]{:S(2)}) async-start(bf16[2,128,4096]{2,0,1:T(2,128)(2,1)} %broadcast_select_fusion), calls=%async_computation | async-start | bytes 4194304 | tf_op jit(solution)/shard_map/all_to_all | solution.py:115
  24.4 0.7 all-gather.4.cloned.1.call-update
  25.1 0.2 all-gather.6.cloned.1.call-start
  25.3 0.5 all-gather.6.cloned.1.call-update
  25.9 39.6 %all-to-all-done = bf16[2,128,4096]{2,0,1:T(2,128)(2,1)} async-done(((bf16[2,128,4096]{2,0,1:T(2,128)(2,1)}), bf16[2,128,4096]{2,0,1:T(2,128)(2,1)}, u32[]{:S(2)}, u32[]{:S(2)}) %all-to-all-start) | async-done | bytes 2097184 | tf_op jit(solution)/shard_map/all_to_all | solution.py:115
  65.5 2.9 %copy.120 = bf16[2,128,4096]{2,1,0:T(8,128)(2,1)S(1)} copy(bf16[2,128,4096]{2,0,1:T(2,128)(2,1)} %all-to-all-done) | data formatting | bytes 4194304 | tf_op jit(solution)/shard_map/all_to_all | solution.py:115
  68.4 10.7 %fusion.29 = f32[2,16,8,384]{3,1,0,2:T(8,128)S(1)} fusion(bf16[8,4096,384]{2,1,0:T(8,128)(2,1)} %param.28, bf16[2,16,8,4096]{3,2,1,0:T(8,128)(2,1)S(1)} %bitcast.84), kind=kOutput, calls=%fused_computation.39 | convolution fusion | flops 805306368 | bytes 27656192 | tf_op jit(solution)/shard_map/csed,edf->csef/dot_general | solution.py:118
  79.1 21.4 %fusion.20 = bf16[2,16,8,4096]{3,1,0,2:T(8,128)(2,1)} fusion(bf16[8,384,4096]{2,1,0:T(8,128)(2,1)} %param.30, bf16[8,4096,384]{2,1,0:T(8,128)(2,1)} %param.29, bf16[2,16,8,4096]{3,2,1,0:T(8,128)(2,1)S(1)} %bitcast.85, f32[2,16,8,384]{3,1,0,2:T(8,128)S(1)} %fusion.29), kind=kOutput, calls=%fused_computation.25 | convolution fusion | flops 1612251136 | bytes 54919168 | tf_op jit(solution)/shard_map/csef,efd->csed/dot_general | solution.py:124
  100.5 2.7 %copy.119 = bf16[2,16,8,4096]{3,2,1,0:T(8,128)(2,1)S(1)} copy(bf16[2,16,8,4096]{3,1,0,2:T(8,128)(2,1)} %fusion.20) | data formatting | bytes 4194304 | tf_op jit(solution)/shard_map/convert_element_type | solution.py:125
  103.3 3.5 %copy.90 = bf16[2,128,4096]{2,0,1:T(2,128)(2,1)} copy(bf16[2,128,4096]{2,1,0:T(8,128)(2,1)S(1)} %bitcast.87) | data formatting | bytes 4194304 | tf_op jit(solution)/shard_map/reshape | solution.py:126
  106.8 11.5 %all-to-all-start.1 = ((bf16[2,128,4096]{2,0,1:T(2,128)(2,1)}), bf16[2,128,4096]{2,0,1:T(2,128)(2,1)}, u32[]{:S(2)}, u32[]{:S(2)}) async-start(bf16[2,128,4096]{2,0,1:T(2,128)(2,1)} %copy.90), calls=%async_computation.1 | async-start | bytes 4194304 | tf_op jit(solution)/shard_map/all_to_all | solution.py:128
  118.3 0.3 all-gather.8.cloned.1.call-start
  118.5 0.5 all-gather.8.cloned.1.call-update
  119.0 0.1 reshape.194
  119.2 0.1 copy.79
  119.4 0.1 fusion.62
  119.5 0.1 fusion.59
  119.7 0.1 fusion.64
  119.8 57.6 %all_gather.15 = bf16[512,4,128]{2,0,1:T(8,128)(2,1)S(1)} all-gather(bf16[128,4,128]{2,0,1:T(8,128)(2,1)S(1)} %fusion.64), channel_id=1, replica_groups=mesh['grp'=2,'ep'=4,'tp'=4] {'ep'}, dimensions={0}, use_global_device_ids=true | all-gather | bytes 655360 | tf_op jit(solution)/shard_map/all_gather | solution.py:34
  177.5 15.9 %all_gather.16 = bf16[512,4,128]{2,0,1:T(8,128)(2,1)S(1)} all-gather(bf16[128,4,128]{2,0,1:T(8,128)(2,1)S(1)} %copy.76), channel_id=1, replica_groups=mesh['grp'=2,'ep'=4,'tp'=4] {'ep'}, dimensions={0}, use_global_device_ids=true | all-gather | bytes 655360 | tf_op jit(solution)/shard_map/all_gather | solution.py:35
  193.4 0.1 fusion.61
  193.5 1.5 conditional.1
  193.6 0.5 fusion.75
  194.1 0.4 fusion.5
  194.5 0.2 copy.97
  194.7 0.3 fusion.4
  195.0 0.1 copy.77
  195.2 0.9 fusion.71
  196.0 2.0 fusion.76
  198.0 2.0 fusion.53
  200.1 2.8 %fusion.28 = bf16[128,4096]{1,0:T(8,128)(2,1)S(1)} fusion(bf16[128,4,48]{0,2,1:T(8,128)(2,1)S(1)} %bitcast.90, bf16[4,48,4096]{2,1,0:T(8,128)(2,1)} %bitcast.98), kind=kOutput, calls=%fused_computation.38 | convolution fusion | flops 204996608 | bytes 2670592 | tf_op jit(solution)/shard_map/rnp,npd->nrd/dot_general | solution.py:80
  202.9 2.9 %copy.91 = bf16[2,128,4096]{2,1,0:T(8,128)(2,1)S(1)} copy(bf16[2,128,4096]{2,0,1:T(2,128)(2,1)} %all-to-all-done.1) | data formatting | bytes 4194304 | tf_op jit(solution)/shard_map/all_to_all | solution.py:128
  205.8 3.2 %gather_fusion.1 = bf16[256,4096]{1,0:T(8,128)(2,1)} fusion(bf16[256,4096]{1,0:T(8,128)(2,1)S(1)} %bitcast.83, s32[1024]{0:T(1024)S(1)} %pad_clamp_fusion), kind=kCustom, calls=%fused_computation.1 | custom fusion | bytes 4195328 | tf_op jit(solution)/shard_map/gather | solution.py:129
  209.0 5.4 %reshape.195 = f32[128,2,4096]{2,1,0:T(2,128)} reshape(bf16[256,4096]{1,0:T(8,128)(2,1)} %gather_fusion.1) | data formatting | bytes 6291456 | tf_op jit(solution)/shard_map/convert_element_type | solution.py:130
  214.4 8.7 %multiply_reduce_fusion = f32[128,4096]{1,0:T(8,128)S(1)} fusion(f32[128,2,4096]{2,1,0:T(2,128)} %reshape.195, f32[128,2]{1,0:T(8,128)S(1)} %copy.79), kind=kLoop, calls=%fused_computation.26 | loop fusion | flops 1572864 | bytes 6292480 | tf_op jit(solution)/shard_map/reduce_sum | solution.py:130
  223.2 1.2 add_convert_fusion
  (48 shorter events, 0.5 us)
Async XLA Ops:
  7.2 3.7 %copy-start = (bf16[128,4096]{1,0:T(8,128)(2,1)S(1)}, bf16[128,4096]{1,0:T(8,128)(2,1)}, u32[]{:S(2)}) copy-start(bf16[128,4096]{1,0:T(8,128)(2,1)} %param.24) | copy-start | bytes 3145732
  7.2 3.7 %copy-start.6 = (f32[4096]{0:T(1024)S(1)}, f32[4096]{0:T(1024)}, u32[]{:S(2)}) copy-start(f32[4096]{0:T(1024)} %param.25) | copy-start | bytes 49156
  8.1 2.7 %copy-start.1 = (s32[128,2]{1,0:T(8,128)}, s32[128,2]{1,0:T(8,128)S(1)}, u32[]{:S(2)}) copy-start(s32[128,2]{1,0:T(8,128)S(1)} %copy.80) | copy-start | bytes 3076
  16.9 48.5 %all-to-all-start = ((bf16[2,128,4096]{2,0,1:T(2,128)(2,1)}), bf16[2,128,4096]{2,0,1:T(2,128)(2,1)}, u32[]{:S(2)}, u32[]{:S(2)}) async-start(bf16[2,128,4096]{2,0,1:T(2,128)(2,1)} %broadcast_select_fusion), calls=%async_computation | async-start | bytes 4194304 | tf_op jit(solution)/shard_map/all_to_all | solution.py:115
  24.4 171.6 %all-gather.4.cloned.1.call-start = ((), (), s32[]{:S(2)}) async-start(), calls=%async_computation.2 | async-start | bytes 1966080 | tf_op jit(solution)/shard_map/all_gather | solution.py:69
  25.1 172.9 %all-gather.6.cloned.1.call-start = ((), (), s32[]{:S(2)}) async-start(), calls=%async_computation.3 | async-start | bytes 1966080 | tf_op jit(solution)/shard_map/all_gather | solution.py:70
  106.8 12.3 %copy-start.2 = (s32[128,2]{1,0:T(8,128)S(1)}, s32[128,2]{1,0:T(8,128)}, u32[]{:S(2)}) copy-start(s32[128,2]{1,0:T(8,128)} %copy-done.1) | copy-start | bytes 3076
  106.8 12.4 %copy-start.7 = (f32[128,2]{0,1:T(2,128)S(1)}, f32[128,2]{0,1:T(2,128)}, u32[]{:S(2)}) copy-start(f32[128,2]{0,1:T(2,128)} %param.27) | copy-start | bytes 3076
  106.8 12.5 %copy-start.5 = (bf16[128,4,128]{2,1,0:T(4,128)(2,1)S(1)}, bf16[128,4,128]{2,1,0:T(4,128)(2,1)}, u32[]{:S(2)}) copy-start(bf16[128,4,128]{2,1,0:T(4,128)(2,1)} %param.20) | copy-start | bytes 393220
  106.8 12.6 %copy-start.10 = (f32[512,4]{0,1:T(4,128)S(1)}, f32[512,4]{0,1:T(4,128)}, u32[]{:S(2)}) copy-start(f32[512,4]{0,1:T(4,128)} %param.21) | copy-start | bytes 24580
  106.8 12.6 %copy-start.3 = (bf16[128,4,128]{2,1,0:T(4,128)(2,1)S(1)}, bf16[128,4,128]{2,1,0:T(4,128)(2,1)}, u32[]{:S(2)}) copy-start(bf16[128,4,128]{2,1,0:T(4,128)(2,1)} %param.19) | copy-start | bytes 393220
  106.8 12.7 %copy-start.4 = (bf16[128,4,128]{2,1,0:T(4,128)(2,1)S(1)}, bf16[128,4,128]{2,1,0:T(4,128)(2,1)}, u32[]{:S(2)}) copy-start(bf16[128,4,128]{2,1,0:T(4,128)(2,1)} %param.18) | copy-start | bytes 393220
  106.8 12.9 %copy-start.8 = (f32[128]{0:T(128)S(1)}, f32[128]{0:T(128)}, u32[]{:S(2)}) copy-start(f32[128]{0:T(128)} %param.23) | copy-start | bytes 1540
  106.8 96.0 %all-to-all-start.1 = ((bf16[2,128,4096]{2,0,1:T(2,128)(2,1)}), bf16[2,128,4096]{2,0,1:T(2,128)(2,1)}, u32[]{:S(2)}, u32[]{:S(2)}) async-start(bf16[2,128,4096]{2,0,1:T(2,128)(2,1)} %copy.90), calls=%async_computation.1 | async-start | bytes 4194304 | tf_op jit(solution)/shard_map/all_to_all | solution.py:128
  118.3 75.1 %copy-start.9 = (f32[128]{0:T(128)S(1)}, f32[128]{0:T(128)}, u32[]{:S(2)}) copy-start(f32[128]{0:T(128)} %param.22) | copy-start | bytes 1540
  118.3 81.8 %all-gather.8.cloned.1.call-start = ((), (), s32[]{:S(2)}) async-start(), calls=%async_computation.4 | async-start | bytes 1966080 | tf_op jit(solution)/shard_map/all_gather | solution.py:71
Sparse Core Ops, SparseCore 0:
  26.8 28.5 all-gather.3
  56.9 20.2 all-gather.5
  120.6 28.3 all-gather.7
where the time goes:
time: 231 us
  blocking collectives  73.5 us (32%)
  waiting for transfers between devices  41.3 us (18%)
  matrix products  39.7 us (17%)
  local copies, waits for them, and re-layouts  24.6 us (11%)
  starting transfers between devices  19.4 us (8%)
  other arithmetic  18.3 us (8%)
  between operations  14.1 us (6%)
    all_gather x1, blocking collectives, attend(): key_part = lax.all_gather(key_norm, 'ep', axis=0, tiled=True)  57.6 us
    all_to_all x1, waiting for transfers between devices, mixture(): lax.all_to_all(outgoing, ('ep', 'tp'), split_axis=1, concat_axis=1, tiled...  39.6 us
    dot_general x1, matrix products, mixture(): jnp.einsum('csef,efd->csed', hidden, expert_down, preferred_element_type=...  21.4 us
    all_gather x1, blocking collectives, attend(): value_part = lax.all_gather(values, 'ep', axis=0, tiled=True)  15.9 us
    all_to_all x1, starting transfers between devices, mixture(): lax.all_to_all(produced, ('ep', 'tp'), split_axis=1, concat_axis=1, tiled...  11.5 us
    dot_general x1, matrix products, mixture(): jnp.einsum('csed,edf->csef', grouped, expert_gate, preferred_element_type...  10.7 us
    reduce_sum x1, other arithmetic, mixture(): jnp.sum(route_weights[:, :, None] * picked_rows.astype(jnp.float32), axis=1)  8.75 us
    all_to_all x1, starting transfers between devices, mixture(): lax.all_to_all(outgoing, ('ep', 'tp'), split_axis=1, concat_axis=1, tiled...  7.44 us
  transfers between devices with their start and end apart: 5, of which 1 were waited for; matrix products, arithmetic and copies ran while one was open for 22% of the time, Pallas kernels for 0%

commit v1 on v0

--- a/solution.py
+++ b/solution.py
@@ -1,3 +1,4 @@
+import functools
 import jax
 import jax.numpy as jnp
 from jax import lax
@@ -7,6 +8,16 @@
 EXPERTS = 128
 TOP_K = 2
 CAP = 2
+
+
+def serve_tokens(block_here, mesh_name, d_out, along_dim):
+    frame_out = jax.lax.psum(1, mesh_name)
+    taken_in = jnp.split(block_here, frame_out, d_out)
+    big = jax.lax.all_to_all(jnp.stack(taken_in, axis=0), mesh_name, 0, 0)
+    return jnp.concatenate(big, axis=along_dim)
+
+
+_spread_region = functools.partial(serve_tokens, mesh_name=("ep", "tp"), d_out=1, along_dim=1)
 
 
 def rms_rows(row_values, gain_vector):
@@ -125,7 +136,7 @@
         .astype(jnp.bfloat16)
         .reshape(CAP, -1, D)
     )
-    returned = lax.all_to_all(produced, ("ep", "tp"), split_axis=1, concat_axis=1, tiled=True)
+    returned = _spread_region(produced)
     picked_rows = returned.reshape(CAP * EXPERTS, D)[slot_index].reshape(row_count, TOP_K, D)
     routed = jnp.sum(route_weights[:, :, None] * picked_rows.astype(jnp.float32), axis=1)
     return (shared_out.astype(jnp.float32) + routed).astype(jnp.bfloat16)

time: 231 us -> 240 us (1.039)
  local copies, waits for them, and re-layouts: 24.6 us -> 34 us
    unnamed x26 -> x39, local copies, waits for them, and re-layouts: 1.06 us -> 13.8 us
    all_to_all x1 -> x0, local copies, waits for them, and re-layouts: 2.92 us -> none  [mixture(): lax.all_to_all(produced, ('ep', 'tp'), split_axis=1, concat_axis=1, tiled...]
  transfers between devices with their start and end apart: 5 -> 5, of which waited for: 1 -> 1; matrix products, arithmetic and copies ran while one was open for 22% -> 26% of each run, Pallas kernels for 0% -> 0%
where the time goes in v1:
time: 240 us
  blocking collectives  71.6 us (30%)
  waiting for transfers between devices  41.5 us (17%)
  matrix products  40.4 us (17%)
  local copies, waits for them, and re-layouts  34 us (14%)
  starting transfers between devices  19.1 us (8%)
  other arithmetic  18.9 us (8%)
  between operations  14 us (6%)
    all_gather x1, blocking collectives, attend(): key_part = lax.all_gather(key_norm, 'ep', axis=0, tiled=True)  55.5 us
    all_to_all x1, waiting for transfers between devices, mixture(): lax.all_to_all(outgoing, ('ep', 'tp'), split_axis=1, concat_axis=1, tiled...  39.6 us
    dot_general x1, matrix products, mixture(): jnp.einsum('csef,efd->csed', hidden, expert_down, preferred_element_type=...  21.4 us
    all_gather x1, blocking collectives, attend(): value_part = lax.all_gather(values, 'ep', axis=0, tiled=True)  16.1 us
    unnamed x39, local copies, waits for them, and re-layouts  13.8 us
    all_to_all x1, starting transfers between devices, serve_tokens(): big = jax.lax.all_to_all(jnp.stack(taken_in, axis=0), mesh_name, 0, 0)  11.4 us
    dot_general x1, matrix products, mixture(): jnp.einsum('csed,edf->csef', grouped, expert_gate, preferred_element_type...  10.7 us
    reduce_sum x1, other arithmetic, mixture(): jnp.sum(route_weights[:, :, None] * picked_rows.astype(jnp.float32), axis=1)  8.75 us
  transfers between devices with their start and end apart: 5, of which 1 were waited for; matrix products, arithmetic and copies ran while one was open for 26% of the time, Pallas kernels for 0%

profile of v1, /device:TPU:0, one launch (start us, length us, event | category | flops | bytes accessed | tf_op | source)
XLA Modules:
  0.0 239.7 jit_solution(6207425893383146032)
XLA Ops:
  7.2 0.9 copy.94
  9.2 1.5 fusion.23
  11.2 1.8 gather_fusion
  13.1 3.8 %broadcast_select_fusion = bf16[2,128,4096]{2,0,1:T(2,128)(2,1)} fusion(pred[2,128]{0,1:T(8,128)(4,1)S(1)} %copy.98, bf16[2,128,4096]{2,1,0:T(8,128)(2,1)S(1)} %bitcast.167), kind=kLoop, calls=%fused_computation.27 | loop fusion | flops 1048576 | bytes 4194560 | tf_op jit(solution)/shard_map/jit(_where)/select_n | solution.py:123
  16.9 7.4 %all-to-all-start = ((bf16[2,128,4096]{2,0,1:T(2,128)(2,1)}), bf16[2,128,4096]{2,0,1:T(2,128)(2,1)}, u32[]{:S(2)}, u32[]{:S(2)}) async-start(bf16[2,128,4096]{2,0,1:T(2,128)(2,1)} %broadcast_select_fusion), calls=%async_computation | async-start | bytes 4194304 | tf_op jit(solution)/shard_map/all_to_all | solution.py:126
  24.4 0.7 all-gather.4.cloned.1.call-update
  25.3 0.5 all-gather.6.cloned.1.call-update
  25.9 39.6 %all-to-all-done = bf16[2,128,4096]{2,0,1:T(2,128)(2,1)} async-done(((bf16[2,128,4096]{2,0,1:T(2,128)(2,1)}), bf16[2,128,4096]{2,0,1:T(2,128)(2,1)}, u32[]{:S(2)}, u32[]{:S(2)}) %all-to-all-start) | async-done | bytes 2097184 | tf_op jit(solution)/shard_map/all_to_all | solution.py:126
  65.5 2.9 %copy.133 = bf16[2,128,4096]{2,1,0:T(8,128)(2,1)S(1)} copy(bf16[2,128,4096]{2,0,1:T(2,128)(2,1)} %all-to-all-done) | data formatting | bytes 4194304 | tf_op jit(solution)/shard_map/all_to_all | solution.py:126
  68.4 10.7 %fusion.29 = f32[2,16,8,384]{3,1,0,2:T(8,128)S(1)} fusion(bf16[8,4096,384]{2,1,0:T(8,128)(2,1)} %param.28, bf16[2,16,8,4096]{3,2,1,0:T(8,128)(2,1)S(1)} %bitcast.149), kind=kOutput, calls=%fused_computation.39 | convolution fusion | flops 805306368 | bytes 27656192 | tf_op jit(solution)/shard_map/csed,edf->csef/dot_general | solution.py:129
  79.1 21.4 %fusion.20 = bf16[2,16,8,4096]{3,1,0,2:T(8,128)(2,1)} fusion(bf16[8,384,4096]{2,1,0:T(8,128)(2,1)} %param.30, bf16[8,4096,384]{2,1,0:T(8,128)(2,1)} %param.29, bf16[2,16,8,4096]{3,2,1,0:T(8,128)(2,1)S(1)} %bitcast.150, f32[2,16,8,384]{3,1,0,2:T(8,128)S(1)} %fusion.29), kind=kOutput, calls=%fused_computation.25 | convolution fusion | flops 1612251136 | bytes 54919168 | tf_op jit(solution)/shard_map/csef,efd->csed/dot_general | solution.py:135
  100.5 2.7 %copy.132 = bf16[2,16,8,4096]{3,2,1,0:T(8,128)(2,1)S(1)} copy(bf16[2,16,8,4096]{3,1,0,2:T(8,128)(2,1)} %fusion.20) | data formatting | bytes 4194304 | tf_op jit(solution)/shard_map/convert_element_type | solution.py:136
  103.3 0.6 fusion.83
  103.9 0.7 fusion.82
  104.6 0.7 fusion.81
  105.2 0.7 fusion.80
  105.9 0.7 fusion.79
  106.6 0.6 fusion.78
  107.2 0.7 fusion.77
  107.9 0.7 fusion.76
  108.5 0.7 fusion.75
  109.2 0.7 fusion.74
  109.9 0.7 fusion.73
  110.5 0.7 fusion.72
  111.2 0.7 fusion.71
  111.8 0.7 fusion.70
  112.5 0.6 fusion.69
  113.1 0.7 fusion.68
  113.8 11.4 %all-to-all-start.1 = ((bf16[16,2,8,4096]{3,2,1,0:T(8,128)(2,1)}), bf16[16,2,8,4096]{3,2,1,0:T(8,128)(2,1)S(1)}, u32[]{:S(2)}, u32[]{:S(2)}) async-start(bf16[16,2,8,4096]{3,2,1,0:T(8,128)(2,1)} %fusion.68), calls=%async_computation.1 | async-start | bytes 4194304 | tf_op jit(solution)/shard_map/all_to_all | solution.py:16
  125.3 0.7 all-gather.8.cloned.1.call-update
  126.1 0.7 copy.93
  126.9 0.9 copy.90
  127.8 0.7 dynamic-slice_bitcast_fusion
  128.9 55.5 %all_gather.15 = bf16[512,4,128]{2,0,1:T(8,128)(2,1)S(1)} all-gather(bf16[128,4,128]{2,0,1:T(8,128)(2,1)S(1)} %fusion.64), channel_id=1, replica_groups=mesh['grp'=2,'ep'=4,'tp'=4] {'ep'}, dimensions={0}, use_global_device_ids=true | all-gather | bytes 655360 | tf_op jit(solution)/shard_map/all_gather | solution.py:45
  184.5 16.1 %all_gather.16 = bf16[512,4,128]{2,0,1:T(8,128)(2,1)S(1)} all-gather(bf16[128,4,128]{2,0,1:T(8,128)(2,1)S(1)} %copy.90), channel_id=1, replica_groups=mesh['grp'=2,'ep'=4,'tp'=4] {'ep'}, dimensions={0}, use_global_device_ids=true | all-gather | bytes 655360 | tf_op jit(solution)/shard_map/all_gather | solution.py:46
  200.6 0.8 fusion.61
  201.4 2.2 conditional.1
  201.5 1.2 fusion.91
  203.7 0.9 fusion.87
  204.6 2.0 fusion.92
  206.6 2.0 fusion.53
  208.6 2.8 %fusion.28 = bf16[128,4096]{1,0:T(8,128)(2,1)S(1)} fusion(bf16[128,4,48]{0,2,1:T(8,128)(2,1)S(1)} %bitcast.171, bf16[4,48,4096]{2,1,0:T(8,128)(2,1)} %bitcast.179), kind=kOutput, calls=%fused_computation.38 | convolution fusion | flops 204996608 | bytes 2670592 | tf_op jit(solution)/shard_map/rnp,npd->nrd/dot_general | solution.py:91
  211.5 1.3 copy-done
  212.8 1.7 copy.104
  214.5 3.2 %gather_fusion.1 = bf16[256,4096]{1,0:T(8,128)(2,1)} fusion(bf16[256,4096]{1,0:T(8,128)(2,1)S(1)} %bitcast.148, s32[1024]{0:T(1024)S(1)} %pad_clamp_fusion), kind=kCustom, calls=%fused_computation.1 | custom fusion | bytes 4195328 | tf_op jit(solution)/shard_map/gather | solution.py:140
  217.7 5.5 %reshape.195 = f32[128,2,4096]{2,1,0:T(2,128)} reshape(bf16[256,4096]{1,0:T(8,128)(2,1)} %gather_fusion.1) | data formatting | bytes 6291456 | tf_op jit(solution)/shard_map/convert_element_type | solution.py:141
  223.2 8.7 %multiply_reduce_fusion = f32[128,4096]{1,0:T(8,128)S(1)} fusion(f32[128,2,4096]{2,1,0:T(2,128)} %reshape.195, f32[128,2]{1,0:T(8,128)S(1)} %copy-done.6), kind=kLoop, calls=%fused_computation.26 | loop fusion | flops 1572864 | bytes 6292480 | tf_op jit(solution)/shard_map/reduce_sum | solution.py:141
  231.9 1.2 add_convert_fusion
  (61 shorter events, 3.7 us)
Async XLA Ops:
  7.2 3.7 %copy-start.1 = (bf16[128,4096]{1,0:T(8,128)(2,1)S(1)}, bf16[128,4096]{1,0:T(8,128)(2,1)}, u32[]{:S(2)}) copy-start(bf16[128,4096]{1,0:T(8,128)(2,1)} %param.24) | copy-start | bytes 3145732
  7.2 3.7 %copy-start.7 = (f32[4096]{0:T(1024)S(1)}, f32[4096]{0:T(1024)}, u32[]{:S(2)}) copy-start(f32[4096]{0:T(1024)} %param.25) | copy-start | bytes 49156
  8.1 2.7 %copy-start.2 = (s32[128,2]{1,0:T(8,128)}, s32[128,2]{1,0:T(8,128)S(1)}, u32[]{:S(2)}) copy-start(s32[128,2]{1,0:T(8,128)S(1)} %copy.94) | copy-start | bytes 3076
  16.9 48.5 %all-to-all-start = ((bf16[2,128,4096]{2,0,1:T(2,128)(2,1)}), bf16[2,128,4096]{2,0,1:T(2,128)(2,1)}, u32[]{:S(2)}, u32[]{:S(2)}) async-start(bf16[2,128,4096]{2,0,1:T(2,128)(2,1)} %broadcast_select_fusion), calls=%async_computation | async-start | bytes 4194304 | tf_op jit(solution)/shard_map/all_to_all | solution.py:126
  24.4 180.2 %all-gather.4.cloned.1.call-start = ((), (), s32[]{:S(2)}) async-start(), calls=%async_computation.2 | async-start | bytes 1966080 | tf_op jit(solution)/shard_map/all_gather | solution.py:80
  25.1 181.5 %all-gather.6.cloned.1.call-start = ((), (), s32[]{:S(2)}) async-start(), calls=%async_computation.3 | async-start | bytes 1966080 | tf_op jit(solution)/shard_map/all_gather | solution.py:81
  113.8 12.2 %copy-start.3 = (s32[128,2]{1,0:T(8,128)S(1)}, s32[128,2]{1,0:T(8,128)}, u32[]{:S(2)}) copy-start(s32[128,2]{1,0:T(8,128)} %copy-done.2) | copy-start | bytes 3076
  113.8 12.3 %copy-start.8 = (f32[128,2]{0,1:T(2,128)S(1)}, f32[128,2]{0,1:T(2,128)}, u32[]{:S(2)}) copy-start(f32[128,2]{0,1:T(2,128)} %param.27) | copy-start | bytes 3076
  113.8 14.7 %copy-start.4 = (bf16[128,4,128]{2,1,0:T(4,128)(2,1)S(1)}, bf16[128,4,128]{2,1,0:T(4,128)(2,1)}, u32[]{:S(2)}) copy-start(bf16[128,4,128]{2,1,0:T(4,128)(2,1)} %param.19) | copy-start | bytes 393220
  113.8 14.8 %copy-start.5 = (bf16[128,4,128]{2,1,0:T(4,128)(2,1)S(1)}, bf16[128,4,128]{2,1,0:T(4,128)(2,1)}, u32[]{:S(2)}) copy-start(bf16[128,4,128]{2,1,0:T(4,128)(2,1)} %param.18) | copy-start | bytes 393220
  113.8 15.0 %copy-start.9 = (f32[128]{0:T(128)S(1)}, f32[128]{0:T(128)}, u32[]{:S(2)}) copy-start(f32[128]{0:T(128)} %param.23) | copy-start | bytes 1540
  113.8 97.6 %all-to-all-start.1 = ((bf16[16,2,8,4096]{3,2,1,0:T(8,128)(2,1)}), bf16[16,2,8,4096]{3,2,1,0:T(8,128)(2,1)S(1)}, u32[]{:S(2)}, u32[]{:S(2)}) async-start(bf16[16,2,8,4096]{3,2,1,0:T(8,128)(2,1)} %fusion.68), calls=%async_computation.1 | async-start | bytes 4194304 | tf_op jit(solution)/shard_map/all_to_all | solution.py:16
  125.2 83.4 %all-gather.8.cloned.1.call-start = ((), (), s32[]{:S(2)}) async-start(), calls=%async_computation.4 | async-start | bytes 1966080 | tf_op jit(solution)/shard_map/all_gather | solution.py:82
  211.4 1.4 copy-start
  217.7 5.5 %copy-start.6 = (f32[128,2]{1,0:T(8,128)S(1)}, f32[128,2]{1,0:T(8,128)}, u32[]{:S(2)}) copy-start(f32[128,2]{1,0:T(8,128)} %copy.93) | copy-start | bytes 3076
Sparse Core Ops, SparseCore 0:
  26.8 28.5 all-gather.3
  56.9 20.2 all-gather.5
  127.6 28.3 all-gather.7
